TPU v7x, 128 devices: a whole 4x4x4 slice. The times are simulated.
128 devices in a mesh: sp: 16 (over z, x), tp: 8 (over y, core).
Axes of the slice: x: 4, y: 4, z: 4, core: 2. Of those that a mesh axis runs over, the one named last changes fastest.
Arguments:
- stream: bfloat16 [16384, 2048], P(('sp', 'tp')), may hold values from -6 to 6
- projected: bfloat16 [16384, 2048], P('sp', 'tp'), may hold values from -6 to 6
- segments: int32 [16384], P('sp'), may hold values from 0 to 7, never falling along the last dimension, each value on 1 to 3072 neighbouring positions
- group_weight: bfloat16 [4, 512, 512], replicated, may hold values from -0.25 to 0.25
- group_scale: float32 [2048], replicated, may hold values from 0.1 to 1.9
- out_weight: bfloat16 [2048, 2048], replicated, may hold values from -0.125 to 0.125
- ffn_gain: float32 [2048], replicated, may hold values from 0.1 to 1.9
- routes: int32 [16384, 4], P(('sp', 'tp')), may hold values from 0 to 127, all different within a row; in each aligned block of 128 rows (0 to 127, 128 to 255, ...) at most 6 rows name the same one
- route_weights: float32 [16384, 4], P(('sp', 'tp')), may hold values from 0.05 to 0.5
- expert_gate: bfloat16 [128, 2048, 1024], P(('sp', 'tp')), may hold values from -0.25 to 0.25
- expert_up: bfloat16 [128, 2048, 1024], P(('sp', 'tp')), may hold values from -0.25 to 0.25
- expert_down: bfloat16 [128, 1024, 2048], P(('sp', 'tp')), may hold values from -0.1875 to 0.1875
Outputs:
- combined: bfloat16 [16384, 2048], P(('sp', 'tp'))
Inputs may be any that keep to these rules, and one draw needn't show every extreme that they name: `segments`: document numbers never fall along the positions; a document has 1 to 3072 positions, and one has exactly 3072. `routes`: each row names 4 different experts. Among the 128 rows of one device (aligned blocks), no expert is named more than 6 times, and in some blocks one is named exactly 6 times.
All inputs are finite; a program needn't handle non-finite values.
Results may differ from a plain program's by a relative error of at most 0.015.
Values may be sent and summed in bfloat16 or wider, within the bound.
A program may use at most 128 MiB of HBM per device.

v0:
```python
import jax
import jax.numpy as jnp
from jax import lax
from jax.sharding import PartitionSpec as P

GROUPS = 4


norm_eps = 1e-05
clamp_limit = 7.0
sigmoid_alpha = 1.702
longest_window = 16


def sent_to_all(value, axis):
    devices = lax.axis_size(axis)
    return lax.all_to_all(
        jnp.broadcast_to(value[None], (devices, *value.shape)), axis, 0, 0, tiled=True
    )


def joined_by_halves(pieces, combine):
    while len(jax.tree.leaves(pieces)[0]) > 1:
        pieces = jax.vmap(combine)(
            *(jax.tree.map(lambda part: part[side::2], pieces) for side in (0, 1))
        )
    return jax.tree.map(lambda part: part[0], pieces)


def prefix(value, axis, combine, identity):
    devices, index = (lax.axis_size(axis), lax.axis_index(axis))
    passed = jnp.arange(devices) < index

    def kept(part, zero, own):
        part = jnp.where(
            passed.reshape(-1, *(1 for _ in own.shape)), part, jnp.asarray(zero, own.dtype)
        )
        return part

    pieces = jax.tree.map(lambda part: sent_to_all(part, axis), value)
    return joined_by_halves(jax.tree.map(kept, pieces, identity, value), combine)


def rms_scale(resid, gain):
    values = resid.astype(jnp.float32)
    inverse = lax.rsqrt(jnp.mean(values * values, -1, keepdims=True) + norm_eps)
    return (values * inverse * gain).astype(jnp.bfloat16)


def run_expert(block, gate_matrix, up_matrix, down_matrix):
    leading = block.shape[:-1]
    flat_rows = block.reshape(-1, block.shape[-1])
    gate_value = jnp.dot(flat_rows, gate_matrix, preferred_element_type=jnp.float32)
    up_value = jnp.dot(flat_rows, up_matrix, preferred_element_type=jnp.float32)
    gated = jnp.minimum(gate_value, clamp_limit)
    linear = jnp.clip(up_value, -clamp_limit, clamp_limit)
    activated = (gated * jax.nn.sigmoid(sigmoid_alpha * gated) * (linear + 1.0)).astype(
        jnp.bfloat16
    )
    result = jnp.dot(activated, down_matrix, preferred_element_type=jnp.float32).astype(
        jnp.bfloat16
    )
    return result.reshape(leading + (down_matrix.shape[1],))


def keep_latter(earlier, latter):
    present = latter[1] >= 0
    return (
        jnp.where(present[..., None], latter[0], earlier[0]),
        jnp.where(present, latter[1], earlier[1]),
    )


def body(
    stream,
    projected,
    segments,
    group_weight,
    group_scale,
    out_weight,
    ffn_gain,
    routes,
    route_weights,
    expert_gate,
    expert_up,
    expert_down,
):
    row_count, channels = projected.shape
    tp_count = lax.axis_size("tp")
    sp_count = lax.axis_size("sp")
    model_width = channels * tp_count
    group_width = model_width // GROUPS
    rim_rows = longest_window - 1
    channel = lax.axis_index("tp") * channels + jnp.arange(channels, dtype=jnp.int32)
    window = jnp.left_shift(jnp.full((channels,), 2, jnp.int32), channel // group_width)
    identity = (jnp.zeros((rim_rows, channels), jnp.bfloat16), jnp.full((rim_rows,), -1, jnp.int32))
    before_rows, before_docs = prefix(
        (projected[row_count - rim_rows :], segments[row_count - rim_rows :]),
        "sp",
        keep_latter,
        identity,
    )
    extended = jnp.concatenate([before_rows, projected], 0)
    extended_docs = jnp.concatenate([before_docs, segments], 0)
    window_sum = jnp.zeros((row_count, channels), jnp.float32)
    window_count = jnp.zeros((row_count, channels), jnp.float32)
    for offset in range(longest_window):
        earlier_rows = extended[rim_rows - offset : rim_rows - offset + row_count].astype(
            jnp.float32
        )
        earlier_docs = extended_docs[rim_rows - offset : rim_rows - offset + row_count]
        included = (earlier_docs == segments)[:, None] & (offset < window)[None, :]
        window_sum = window_sum + jnp.where(included, earlier_rows, jnp.float32(0.0))
        window_count = window_count + included.astype(jnp.float32)
    mixed = (window_sum / window_count - projected.astype(jnp.float32)).astype(jnp.bfloat16)
    tokens_here = lax.all_to_all(mixed, "tp", split_axis=0, concat_axis=1, tiled=True)
    tok_count = tokens_here.shape[0]
    grouped = jnp.einsum(
        "rgc,gcd->rgd",
        tokens_here.reshape(tok_count, GROUPS, group_width),
        group_weight,
        preferred_element_type=jnp.float32,
    ).reshape(tok_count, model_width)
    scaled = (grouped * group_scale).astype(jnp.bfloat16)
    mixer_out = jnp.dot(scaled, out_weight, preferred_element_type=jnp.float32)
    resid = (stream.astype(jnp.float32) + mixer_out).astype(jnp.bfloat16)
    normed = rms_scale(resid, ffn_gain)
    top_count = routes.shape[1]
    expert_count = sp_count * tp_count
    capacity = 3 * tok_count * top_count // (2 * expert_count)
    flat_routes = routes.reshape(-1)
    onehot = (flat_routes[:, None] == jnp.arange(expert_count, dtype=jnp.int32)[None, :]).astype(
        jnp.int32
    )
    ranking = jnp.sum((jnp.cumsum(onehot, 0) - onehot) * onehot, 1)
    slot_index = flat_routes * capacity + ranking
    token_of = jnp.arange(flat_routes.shape[0], dtype=jnp.int32) // top_count
    slot_token = jnp.zeros((expert_count * capacity,), jnp.int32).at[slot_index].set(token_of)
    slot_live = jnp.zeros((expert_count * capacity,), jnp.bool_).at[slot_index].set(True)
    outgoing = jnp.where(slot_live[:, None], normed[slot_token], jnp.zeros((), jnp.bfloat16))
    results = run_expert(
        lax.all_to_all(
            outgoing.reshape(expert_count, capacity, model_width),
            ("sp", "tp"),
            split_axis=0,
            concat_axis=0,
            tiled=True,
        ),
        expert_gate[0],
        expert_up[0],
        expert_down[0],
    )
    returned = lax.all_to_all(results, ("sp", "tp"), split_axis=0, concat_axis=0, tiled=True)
    picked = returned.reshape(expert_count * capacity, model_width)[slot_index]
    weighted = picked.astype(jnp.float32) * route_weights.reshape(-1)[:, None]
    moe_sum = jnp.sum(weighted.reshape(tok_count, top_count, model_width), 1)
    return (resid.astype(jnp.float32) + moe_sum).astype(jnp.bfloat16)


def solution(mesh):
    in_specs = (
        P(("sp", "tp"), None),
        P("sp", "tp"),
        P("sp"),
        P(),
        P(),
        P(),
        P(),
        P(("sp", "tp"), None),
        P(("sp", "tp"), None),
        P(("sp", "tp"), None, None),
        P(("sp", "tp"), None, None),
        P(("sp", "tp"), None, None),
    )
    out_specs = P(("sp", "tp"), None)
    return jax.shard_map(body, mesh=mesh, in_specs=in_specs, out_specs=out_specs, check_vma=False)
```

profile of v0, /device:TPU:1, one launch (start us, length us, event | category | flops | bytes accessed | tf_op | source)
XLA Modules:
  0.0 230.3 jit_solution(14544700800543057357)
XLA Ops:
  0.0 0.9 slice.154
  0.9 0.6 broadcast_in_dim.99
  1.5 8.4 %all-to-all-start = ((s32[16,1,15]{2,1,0:T(1,128)}), s32[16,1,15]{2,1,0:T(1,128)S(1)}, u32[]{:S(2)}, u32[]{:S(2)}) async-start(s32[16,1,15]{2,1,0:T(1,128)} %broadcast_in_dim.99), calls=%async_computation | async-start | bytes 16384 | tf_op jit(solution)/shard_map/all_to_all | solution.py:17
  10.1 0.8 copy.35
  11.0 0.1 eq.85
  11.1 0.7 broadcast_multiply_fusion
  11.8 0.1 copy.37
  11.9 0.2 fusion.62
  12.3 0.2 fusion.61
  12.5 0.7 slice.164
  13.2 0.1 copy.34
  13.4 2.9 %all-to-all-done = s32[16,1,15]{2,1,0:T(1,128)S(1)} async-done(((s32[16,1,15]{2,1,0:T(1,128)}), s32[16,1,15]{2,1,0:T(1,128)S(1)}, u32[]{:S(2)}, u32[]{:S(2)}) %all-to-all-start) | async-done | bytes 992 | tf_op jit(solution)/shard_map/all_to_all | solution.py:17
  16.3 0.7 broadcast_in_dim.166
  17.0 3.8 %all-to-all-start.1 = ((bf16[16,15,256]{2,1,0:T(8,128)(2,1)}), bf16[16,15,256]{2,1,0:T(8,128)(2,1)S(1)}, u32[]{:S(2)}, u32[]{:S(2)}) async-start(bf16[16,15,256]{2,1,0:T(8,128)(2,1)} %broadcast_in_dim.166), calls=%async_computation.1 | async-start | bytes 262144 | tf_op jit(solution)/shard_map/all_to_all | solution.py:17
  21.0 1.1 fusion.69
  22.2 1.0 fusion.71
  23.2 4.4 %all-to-all-done.1 = bf16[16,15,256]{2,1,0:T(8,128)(2,1)S(1)} async-done(((bf16[16,15,256]{2,1,0:T(8,128)(2,1)}), bf16[16,15,256]{2,1,0:T(8,128)(2,1)S(1)}, u32[]{:S(2)}, u32[]{:S(2)}) %all-to-all-start.1) | async-done | bytes 122912 | tf_op jit(solution)/shard_map/all_to_all | solution.py:17
  28.0 6.1 %fusion.45 = bf16[1024,256]{1,0:T(8,128)(2,1)} fusion(bf16[1024,256]{1,0:T(8,128)(2,1)S(1)} %copy-done.4, bf16[15,256]{1,0:T(8,128)(2,1)S(1)} %fusion.65, f32[256]{0:T(256)S(1)} %fusion.107, pred[256]{0:T(512)(128)(4,1)S(1)} %get-tuple-element.22, pred[256]{0:T(512)(128)(4,1)S(1)} %get-tuple-element.23, pred[256]{0:T(512)(128)(4,1)S(1)} %get-tuple-element.24, ...), kind=kLoop, calls=%fused_computation.100 | loop fusion | flops 36700160 | bytes 1076736 | tf_op jit(solution)/shard_map/convert_element_type | solution.py:115
  34.2 7.4 %all-to-all-start.2 = ((bf16[8,128,256]{2,1,0:T(8,128)(2,1)}), bf16[8,128,256]{2,1,0:T(8,128)(2,1)S(1)}, u32[]{:S(2)}, u32[]{:S(2)}) async-start(bf16[8,128,256]{2,1,0:T(8,128)(2,1)} %bitcast.4), calls=%async_computation.2 | async-start | bytes 1048576 | tf_op jit(solution)/shard_map/all_to_all | solution.py:116
  41.6 2.4 %scatter_custom_fusion.1 = s32[768]{0:T(1024)S(1)} fusion(s32[512]{0:T(512)S(1)} %bitcast.58, s32[512]{0:T(512)S(1)} %add_select_fusion, s32[]{:T(128)} %constant.38.clone.1), kind=kCustom, calls=%fused_computation.207 | custom fusion | bytes 3076 | tf_op jit(solution)/shard_map/scatter | solution.py:138
  44.1 2.4 %scatter_custom_fusion = pred[768]{0:T(1024)(128)(4,1)S(1)} fusion(s32[512]{0:T(512)S(1)} %bitcast.59, pred[512]{0:T(512)(128)(4,1)S(1)} %broadcast.617, pred[]{:T(512)} %constant.33.clone.1), kind=kCustom, calls=%fused_computation.211 | custom fusion | bytes 769 | tf_op jit(solution)/shard_map/scatter | solution.py:139
  46.5 0.2 broadcast_in_dim.170
  46.7 4.2 %all-to-all-done.2 = bf16[8,128,256]{2,1,0:T(8,128)(2,1)S(1)} async-done(((bf16[8,128,256]{2,1,0:T(8,128)(2,1)}), bf16[8,128,256]{2,1,0:T(8,128)(2,1)S(1)}, u32[]{:S(2)}, u32[]{:S(2)}) %all-to-all-start.2) | async-done | bytes 524320 | tf_op jit(solution)/shard_map/all_to_all | solution.py:116
  50.9 1.0 copy.31
  52.0 1.5 convolution_bitcast_fusion
  53.5 0.3 copy.33
  53.9 0.3 fusion.44
  54.2 0.3 copy-done.5
  54.5 4.8 %multiply_reduce_fusion.1 = (f32[128]{0:T(128)S(1)}, f32[128,2048]{1,0:T(8,128)S(1)}) fusion(bf16[128,2048]{0,1:T(8,128)(2,1)S(1)} %fusion.44, bf16[2048,2048]{1,0:T(8,128)(2,1)} %param.17, bf16[128,2048]{1,0:T(8,128)(2,1)S(1)} %copy-done.5), kind=kOutput, calls=%fused_computation.99 | convolution fusion | flops 1075314560 | bytes 10486272 | tf_op jit(solution)/shard_map/dot_general | solution.py:125
  59.3 1.0 copy-done.2
  60.4 0.2 multiply_convert_fusion.1
  60.5 4.3 %gather_fusion = bf16[768,2048]{1,0:T(8,128)(2,1)} fusion(bf16[128,2048]{1,0:T(8,128)(2,1)S(1)} %multiply_convert_fusion.1, s32[1024]{0:T(1024)S(1)} %pad_clamp_fusion.1), kind=kCustom, calls=%fused_computation | custom fusion | bytes 6294528 | tf_op jit(solution)/shard_map/gather | solution.py:140
  64.8 6.2 %gather.9 = bf16[128,6,2048]{2,1,0:T(8,128)(2,1)} reshape(bf16[768,2048]{1,0:T(8,128)(2,1)} %gather_fusion) | data formatting | bytes 6291456 | tf_op jit(solution)/shard_map/gather | solution.py:140
  71.0 2.6 %broadcast_select_fusion = bf16[128,6,2048]{2,1,0:T(8,128)(2,1)S(1)} fusion(bf16[128,6,2048]{2,1,0:T(8,128)(2,1)} %gather.9, pred[128,6]{1,0:T(8,128)(4,1)S(1)} %broadcast_in_dim.170), kind=kLoop, calls=%fused_computation.11 | loop fusion | flops 1572864 | bytes 6292224 | tf_op jit(solution)/shard_map/jit(_where)/select_n | solution.py:140
  73.7 57.7 %all_to_all.40 = bf16[128,6,2048]{2,1,0:T(8,128)(2,1)} all-to-all(bf16[128,6,2048]{2,1,0:T(8,128)(2,1)S(1)} %broadcast_select_fusion), channel_id=1, replica_groups=mesh['sp'=16,'tp'=8] {'sp','tp'}, dimensions={0} | all-to-all | bytes 6291456 | tf_op jit(solution)/shard_map/all_to_all | solution.py:142
  131.3 4.9 %reshape.200 = bf16[768,2048]{1,0:T(8,128)(2,1)S(1)} reshape(bf16[128,6,2048]{2,1,0:T(8,128)(2,1)} %all_to_all.40) | data formatting | bytes 6291456 | tf_op jit(solution)/shard_map/reshape | solution.py:52
  136.2 5.4 %fusion.2 = f32[768,1024]{1,0:T(8,128)S(1)} fusion(bf16[768,2048]{1,0:T(8,128)(2,1)S(1)} %reshape.200, bf16[1,2048,1024]{2,1,0:T(8,128)(2,1)} %param.22), kind=kOutput, calls=%fused_computation.6 | convolution fusion | flops 3221225472 | bytes 10485760 | tf_op jit(solution)/shard_map/dot_general | solution.py:54
  141.6 4.1 %multiply_convert_fusion = bf16[768,1024]{1,0:T(8,128)(2,1)S(1)} fusion(f32[768,1024]{1,0:T(8,128)S(1)} %fusion.2, bf16[768,2048]{1,0:T(8,128)(2,1)S(1)} %reshape.200, bf16[1,2048,1024]{2,1,0:T(8,128)(2,1)S(1)} %copy-done.9), kind=kOutput, calls=%fused_computation.13 | convolution fusion | flops 3229089792 | bytes 12058624 | tf_op jit(solution)/shard_map/dot_general | solution.py:53
  145.8 3.6 %fusion.6 = bf16[768,2048]{1,0:T(8,128)(2,1)S(1)} fusion(bf16[768,1024]{1,0:T(8,128)(2,1)S(1)} %multiply_convert_fusion, bf16[1,1024,2048]{2,1,0:T(8,128)(2,1)S(1)} %copy-done.10), kind=kOutput, calls=%fused_computation.12 | convolution fusion | flops 3222798336 | bytes 8912896 | tf_op jit(solution)/shard_map/dot_general | solution.py:60
  149.4 2.9 %reshape.201 = bf16[128,6,2048]{2,1,0:T(8,128)(2,1)} reshape(bf16[768,2048]{1,0:T(8,128)(2,1)S(1)} %fusion.6) | data formatting | bytes 6291456 | tf_op jit(solution)/shard_map/reshape | solution.py:63
  152.3 5.6 %all-to-all-start.4 = ((bf16[128,6,2048]{2,1,0:T(8,128)(2,1)}), bf16[128,6,2048]{2,1,0:T(8,128)(2,1)}, u32[]{:S(2)}, u32[]{:S(2)}) async-start(bf16[128,6,2048]{2,1,0:T(8,128)(2,1)} %reshape.201), calls=%async_computation.4 | async-start | bytes 8388608 | tf_op jit(solution)/shard_map/all_to_all | solution.py:153
  157.9 0.1 copy.39
  158.0 52.7 %all-to-all-done.4 = bf16[128,6,2048]{2,1,0:T(8,128)(2,1)} async-done(((bf16[128,6,2048]{2,1,0:T(8,128)(2,1)}), bf16[128,6,2048]{2,1,0:T(8,128)(2,1)}, u32[]{:S(2)}, u32[]{:S(2)}) %all-to-all-start.4) | async-done | bytes 3145760 | tf_op jit(solution)/shard_map/all_to_all | solution.py:153
  210.7 4.9 %reshape.202 = bf16[768,2048]{1,0:T(8,128)(2,1)S(1)} reshape(bf16[128,6,2048]{2,1,0:T(8,128)(2,1)} %all-to-all-done.4) | data formatting | bytes 6291456 | tf_op jit(solution)/shard_map/reshape | solution.py:154
  215.6 3.3 %gather_fusion.1 = bf16[512,2048]{1,0:T(8,128)(2,1)} fusion(bf16[768,2048]{1,0:T(8,128)(2,1)S(1)} %reshape.202, s32[1024]{0:T(1024)S(1)} %pad_clamp_fusion), kind=kCustom, calls=%fused_computation.1 | custom fusion | bytes 4196352 | tf_op jit(solution)/shard_map/gather | solution.py:154
  218.9 4.9 %reshape.203 = f32[128,4,2048]{2,1,0:T(4,128)} reshape(bf16[512,2048]{1,0:T(8,128)(2,1)} %gather_fusion.1) | data formatting | bytes 6291456 | tf_op jit(solution)/shard_map/convert_element_type | solution.py:155
  223.8 5.5 %multiply_reduce_fusion = f32[128,2048]{1,0:T(8,128)S(1)} fusion(f32[128,4,2048]{2,1,0:T(4,128)} %reshape.203, f32[128,4]{1,0:T(8,128)S(1)} %copy.39), kind=kLoop, calls=%fused_computation.10 | loop fusion | flops 1835008 | bytes 5244928 | tf_op jit(solution)/shard_map/reduce_sum | solution.py:156
  229.4 0.9 add_convert_fusion
  (65 shorter events, 1.2 us)
Async XLA Ops:
  0.0 52.0 %copy-start = (bf16[4,512,512]{2,1,0:T(8,128)(2,1)S(1)}, bf16[4,512,512]{2,1,0:T(8,128)(2,1)}, u32[]{:S(2)}) copy-start(bf16[4,512,512]{2,1,0:T(8,128)(2,1)} %param.15) | copy-start | bytes 6291460
  0.0 28.0 %copy-start.4 = (bf16[1024,256]{1,0:T(8,128)(2,1)S(1)}, bf16[1024,256]{1,0:T(8,128)(2,1)}, u32[]{:S(2)}) copy-start(bf16[1024,256]{1,0:T(8,128)(2,1)} %param.13) | copy-start | bytes 1572868
  1.5 14.8 %all-to-all-start = ((s32[16,1,15]{2,1,0:T(1,128)}), s32[16,1,15]{2,1,0:T(1,128)S(1)}, u32[]{:S(2)}, u32[]{:S(2)}) async-start(s32[16,1,15]{2,1,0:T(1,128)} %broadcast_in_dim.99), calls=%async_computation | async-start | bytes 16384 | tf_op jit(solution)/shard_map/all_to_all | solution.py:17
  17.0 10.6 %all-to-all-start.1 = ((bf16[16,15,256]{2,1,0:T(8,128)(2,1)}), bf16[16,15,256]{2,1,0:T(8,128)(2,1)S(1)}, u32[]{:S(2)}, u32[]{:S(2)}) async-start(bf16[16,15,256]{2,1,0:T(8,128)(2,1)} %broadcast_in_dim.166), calls=%async_computation.1 | async-start | bytes 262144 | tf_op jit(solution)/shard_map/all_to_all | solution.py:17
  34.2 16.8 %all-to-all-start.2 = ((bf16[8,128,256]{2,1,0:T(8,128)(2,1)}), bf16[8,128,256]{2,1,0:T(8,128)(2,1)S(1)}, u32[]{:S(2)}, u32[]{:S(2)}) async-start(bf16[8,128,256]{2,1,0:T(8,128)(2,1)} %bitcast.4), calls=%async_computation.2 | async-start | bytes 1048576 | tf_op jit(solution)/shard_map/all_to_all | solution.py:116
  51.9 1.9 copy-start.6
  53.5 1.0 copy-start.5
  54.5 5.8 %copy-start.7 = (f32[2048]{0:T(1024)S(1)}, f32[2048]{0:T(1024)}, u32[]{:S(2)}) copy-start(f32[2048]{0:T(1024)} %param.18) | copy-start | bytes 24580
  59.3 1.1 copy-start.2
  136.2 5.4 %copy-start.9 = (bf16[1,2048,1024]{2,1,0:T(8,128)(2,1)S(1)}, bf16[1,2048,1024]{2,1,0:T(8,128)(2,1)}, u32[]{:S(2)}) copy-start(bf16[1,2048,1024]{2,1,0:T(8,128)(2,1)} %param.21) | copy-start | bytes 12582916
  141.6 4.2 %copy-start.10 = (bf16[1,1024,2048]{2,1,0:T(8,128)(2,1)S(1)}, bf16[1,1024,2048]{2,1,0:T(8,128)(2,1)}, u32[]{:S(2)}) copy-start(bf16[1,1024,2048]{2,1,0:T(8,128)(2,1)} %param.23) | copy-start | bytes 12582916
  152.3 5.6 %copy-start.8 = (f32[128,4]{0,1:T(4,128)S(1)}, f32[128,4]{0,1:T(4,128)}, u32[]{:S(2)}) copy-start(f32[128,4]{0,1:T(4,128)} %param.20) | copy-start | bytes 6148
  152.3 58.5 %all-to-all-start.4 = ((bf16[128,6,2048]{2,1,0:T(8,128)(2,1)}), bf16[128,6,2048]{2,1,0:T(8,128)(2,1)}, u32[]{:S(2)}, u32[]{:S(2)}) async-start(bf16[128,6,2048]{2,1,0:T(8,128)(2,1)} %reshape.201), calls=%async_computation.4 | async-start | bytes 8388608 | tf_op jit(solution)/shard_map/all_to_all | solution.py:153
  218.9 11.3 %copy-start.1 = (bf16[4,512,512]{2,1,0:T(8,128)(2,1)S(1)}, bf16[4,512,512]{2,1,0:T(8,128)(2,1)}, u32[]{:S(2)}) copy-start(bf16[4,512,512]{2,1,0:T(8,128)(2,1)} %param.15) | copy-start | bytes 6291460
  223.8 5.5 %copy-start.3 = (f32[128,2048]{1,0:T(8,128)S(1)}, f32[128,2048]{1,0:T(8,128)}, u32[]{:S(2)}) copy-start(f32[128,2048]{1,0:T(8,128)} %copy-done.2) | copy-start | bytes 3145732
where the time goes:
time: 231 us; the launch traced here: 230 us
  waiting for transfers between devices  64.2 us (28%)
  blocking collectives  57.7 us (25%)
  local copies, waits for them, and re-layouts  43.6 us (19%)
  starting transfers between devices  25.2 us (11%)
  other arithmetic  19.7 us (9%)
  matrix products  19.4 us (8%)
    all_to_all x1, blocking collectives, body(): lax.all_to_all(outgoing.reshape(expert_count, capacity, model_width), ('s...  57.7 us
    all_to_all x1, waiting for transfers between devices, body(): lax.all_to_all(results, ('sp', 'tp'), split_axis=0, concat_axis=0, tiled=...  52.7 us
    all_to_all x2, starting transfers between devices, sent_to_all(): lax.all_to_all(jnp.broadcast_to(value[None], (devices, *value.shape)), ax...  12.2 us
    gather x2, local copies, waits for them, and re-layouts, body(): normed[slot_token]  10.5 us
    all_to_all x1, starting transfers between devices, body(): lax.all_to_all(mixed, 'tp', split_axis=0, concat_axis=1, tiled=True)  7.42 us
    all_to_all x2, waiting for transfers between devices, sent_to_all(): lax.all_to_all(jnp.broadcast_to(value[None], (devices, *value.shape)), ax...  7.27 us
    convert_element_type x1, other arithmetic, body(): (window_sum / window_count - projected.astype(jnp.float32)).astype(jnp.bf...  6.15 us
    all_to_all x1, starting transfers between devices, body(): lax.all_to_all(results, ('sp', 'tp'), split_axis=0, concat_axis=0, tiled=...  5.59 us
  transfers between devices with their start and end apart: 4, of which 4 were waited for; matrix products, arithmetic and copies ran while one was open for 5% of the time, Pallas kernels for 0%

commit v1 on v0

--- a/solution.py
+++ b/solution.py
@@ -2,6 +2,8 @@
 import jax.numpy as jnp
 from jax import lax
 from jax.sharding import PartitionSpec as P
+from jax.experimental import pallas as pl
+from jax.experimental.pallas import tpu as pltpu
 
 GROUPS = 4
 
@@ -69,6 +71,60 @@
         jnp.where(present[..., None], latter[0], earlier[0]),
         jnp.where(present, latter[1], earlier[1]),
     )
+
+
+MESH = pl.DeviceIdType.MESH
+
+
+def exchange_kernel(count, tp_count, in_ref, out_ref, send_sem, recv_sem, own_sem):
+    me = lax.axis_index("sp") * tp_count + lax.axis_index("tp")
+    own = pltpu.make_async_copy(in_ref.at[me], out_ref.at[me], own_sem)
+    own.start()
+    barrier = pltpu.get_barrier_semaphore()
+
+    @pl.loop(1, count)
+    def _(step):
+        peer = lax.rem(me + step, count)
+        pl.semaphore_signal(
+            barrier,
+            inc=1,
+            device_id=(peer // tp_count, lax.rem(peer, tp_count)),
+            device_id_type=MESH,
+        )
+
+    pl.semaphore_wait(barrier, count - 1)
+
+    @pl.loop(1, count)
+    def _(step):
+        peer = lax.rem(me + lax.rem(step * 37, count), count)
+        pltpu.make_async_remote_copy(
+            in_ref.at[peer],
+            out_ref.at[me],
+            send_sem,
+            recv_sem,
+            device_id=(peer // tp_count, lax.rem(peer, tp_count)),
+            device_id_type=MESH,
+        ).start()
+
+    rest = pl.ds(0, count - 1)
+    pltpu.make_async_copy(in_ref.at[rest], in_ref.at[rest], send_sem).wait()
+    pltpu.make_async_copy(out_ref.at[rest], out_ref.at[rest], recv_sem).wait()
+    own.wait()
+
+
+def exchange(blocks, name, collective_id):
+    count = blocks.shape[0]
+    return pl.pallas_call(
+        lambda *refs: exchange_kernel(count, lax.axis_size("tp"), *refs),
+        out_shape=jax.ShapeDtypeStruct(blocks.shape, blocks.dtype),
+        in_specs=[pl.BlockSpec(memory_space=pltpu.VMEM)],
+        out_specs=pl.BlockSpec(memory_space=pltpu.VMEM),
+        scratch_shapes=[pltpu.SemaphoreType.DMA] * 3,
+        name=name,
+        compiler_params=pltpu.CompilerParams(
+            collective_id=collective_id, has_side_effects=True, vmem_limit_bytes=16 << 20
+        ),
+    )(blocks)
 
 
 def body(
@@ -138,19 +194,14 @@
     slot_token = jnp.zeros((expert_count * capacity,), jnp.int32).at[slot_index].set(token_of)
     slot_live = jnp.zeros((expert_count * capacity,), jnp.bool_).at[slot_index].set(True)
     outgoing = jnp.where(slot_live[:, None], normed[slot_token], jnp.zeros((), jnp.bfloat16))
+    arrived = exchange(outgoing.reshape(expert_count, capacity * 8, model_width // 8), "dispatch", 0)
     results = run_expert(
-        lax.all_to_all(
-            outgoing.reshape(expert_count, capacity, model_width),
-            ("sp", "tp"),
-            split_axis=0,
-            concat_axis=0,
-            tiled=True,
-        ),
+        arrived.reshape(expert_count * capacity, model_width),
         expert_gate[0],
         expert_up[0],
         expert_down[0],
     )
-    returned = lax.all_to_all(results, ("sp", "tp"), split_axis=0, concat_axis=0, tiled=True)
+    returned = exchange(results.reshape(expert_count, capacity * 8, model_width // 8), "giveback", 1)
     picked = returned.reshape(expert_count * capacity, model_width)[slot_index]
     weighted = picked.astype(jnp.float32) * route_weights.reshape(-1)[:, None]
     moe_sum = jnp.sum(weighted.reshape(tok_count, top_count, model_width), 1)

time: 231 us -> 206 us (0.89)
  Pallas kernels: 0 us -> 88.4 us
  blocking collectives: 57.7 us -> 0 us
  waiting for transfers between devices: 64.2 us -> 11.1 us
  starting transfers between devices: 25.2 us -> 22.1 us
  matrix products: 19.4 us -> 21.8 us
    pallas_call x0 -> x2, Pallas kernels: none -> 88.4 us  [exchange(): pl.pallas_call(lambda *refs: exchange_kernel(count, lax.axis_size('tp'),...]
    all_to_all x1 -> x0, blocking collectives: 57.7 us -> none  [body(): lax.all_to_all(outgoing.reshape(expert_count, capacity, model_width), ('s...]
    all_to_all x1 -> x0, waiting for transfers between devices: 52.7 us -> none  [body(): lax.all_to_all(results, ('sp', 'tp'), split_axis=0, concat_axis=0, tiled=...]
    all_to_all x1 -> x0, starting transfers between devices: 5.59 us -> none  [body(): lax.all_to_all(results, ('sp', 'tp'), split_axis=0, concat_axis=0, tiled=...]
    all_to_all x2, waiting for transfers between devices: 7.27 us -> 4.52 us  [sent_to_all(): lax.all_to_all(jnp.broadcast_to(value[None], (devices, *value.shape)), ax...]
    all_to_all x2, starting transfers between devices: 12.2 us -> 14.9 us  [sent_to_all(): lax.all_to_all(jnp.broadcast_to(value[None], (devices, *value.shape)), ax...]
    all_to_all x1, waiting for transfers between devices: 4.23 us -> 6.62 us  [body(): lax.all_to_all(mixed, 'tp', split_axis=0, concat_axis=1, tiled=True)]
  transfers between devices with their start and end apart: 4 -> 3, of which waited for: 4 -> 3; matrix products, arithmetic and copies ran while one was open for 5% -> 5% of each run, Pallas kernels for 0% -> 0%
where the time goes in v1:
time: 206 us; the launch traced here: 205 us
  Pallas kernels  88.4 us (43%)
  local copies, waits for them, and re-layouts  42.7 us (21%)
  starting transfers between devices  22.1 us (11%)
  matrix products  21.8 us (11%)
  other arithmetic  18.2 us (9%)
  waiting for transfers between devices  11.1 us (5%)
    pallas_call x2, Pallas kernels, exchange(): pl.pallas_call(lambda *refs: exchange_kernel(count, lax.axis_size('tp'),...  88.4 us
    all_to_all x2, starting transfers between devices, sent_to_all(): lax.all_to_all(jnp.broadcast_to(value[None], (devices, *value.shape)), ax...  14.9 us
    gather x2, local copies, waits for them, and re-layouts, body(): normed[slot_token]  8.63 us
    all_to_all x1, starting transfers between devices, body(): lax.all_to_all(mixed, 'tp', split_axis=0, concat_axis=1, tiled=True)  7.13 us
    all_to_all x1, waiting for transfers between devices, body(): lax.all_to_all(mixed, 'tp', split_axis=0, concat_axis=1, tiled=True)  6.62 us
    dot_general x1, matrix products, run_expert(): up_value = jnp.dot(flat_rows, up_matrix, preferred_element_type=jnp.float32)  6.5 us
    convert_element_type x1, other arithmetic, body(): (window_sum / window_count - projected.astype(jnp.float32)).astype(jnp.bf...  6.12 us
    reduce_sum x1, other arithmetic, body(): moe_sum = jnp.sum(weighted.reshape(tok_count, top_count, model_width), 1)  5.5 us
  transfers between devices with their start and end apart: 3, of which 3 were waited for; matrix products, arithmetic and copies ran while one was open for 5% of the time, Pallas kernels for 0%

profile of v1, /device:TPU:1, one launch (start us, length us, event | category | flops | bytes accessed | tf_op | source)
XLA Modules:
  0.0 204.7 jit_solution(17817437648179007124)
XLA Ops:
  0.0 0.9 slice.154
  0.9 0.6 broadcast_in_dim.162
  1.5 8.4 %all-to-all-start = ((s32[16,1,15]{2,1,0:T(1,128)}), s32[16,1,15]{2,1,0:T(1,128)S(1)}, u32[]{:S(2)}, u32[]{:S(2)}) async-start(s32[16,1,15]{2,1,0:T(1,128)} %broadcast_in_dim.162), calls=%async_computation | async-start | bytes 16384 | tf_op jit(solution)/shard_map/all_to_all | solution.py:19
  10.1 0.8 copy.39
  11.1 0.7 broadcast_multiply_fusion
  11.8 0.1 copy.41
  11.9 0.2 fusion.62
  12.3 0.1 copy.38
  12.5 0.2 fusion.61
  12.7 2.4 %scatter_custom_fusion = pred[768]{0:T(1024)(128)(4,1)S(1)} fusion(s32[512]{0:T(512)S(1)} %bitcast.60, pred[512]{0:T(512)(128)(4,1)S(1)} %broadcast.617, pred[]{:T(512)} %constant.33.clone.1), kind=kCustom, calls=%fused_computation.212 | custom fusion | bytes 769 | tf_op jit(solution)/shard_map/scatter | solution.py:195
  15.2 0.2 broadcast_in_dim.174
  15.5 0.7 slice.164
  16.2 0.1 all-to-all-done
  16.3 0.7 broadcast_in_dim.170
  17.0 6.5 %all-to-all-start.1 = ((bf16[16,15,256]{2,1,0:T(8,128)(2,1)}), bf16[16,15,256]{2,1,0:T(8,128)(2,1)S(1)}, u32[]{:S(2)}, u32[]{:S(2)}) async-start(bf16[16,15,256]{2,1,0:T(8,128)(2,1)} %broadcast_in_dim.170), calls=%async_computation.1 | async-start | bytes 262144 | tf_op jit(solution)/shard_map/all_to_all | solution.py:19
  23.8 1.1 fusion.69
  24.9 1.0 fusion.71
  26.0 4.4 %all-to-all-done.1 = bf16[16,15,256]{2,1,0:T(8,128)(2,1)S(1)} async-done(((bf16[16,15,256]{2,1,0:T(8,128)(2,1)}), bf16[16,15,256]{2,1,0:T(8,128)(2,1)S(1)}, u32[]{:S(2)}, u32[]{:S(2)}) %all-to-all-start.1) | async-done | bytes 122912 | tf_op jit(solution)/shard_map/all_to_all | solution.py:19
  30.8 6.1 %fusion.45 = bf16[1024,256]{1,0:T(8,128)(2,1)} fusion(bf16[1024,256]{1,0:T(8,128)(2,1)S(1)} %copy-done.6, bf16[15,256]{1,0:T(8,128)(2,1)S(1)} %fusion.65, f32[256]{0:T(256)S(1)} %fusion.107, pred[256]{0:T(512)(128)(4,1)S(1)} %get-tuple-element.22, pred[256]{0:T(512)(128)(4,1)S(1)} %get-tuple-element.23, pred[256]{0:T(512)(128)(4,1)S(1)} %get-tuple-element.24, ...), kind=kLoop, calls=%fused_computation.100 | loop fusion | flops 36700160 | bytes 1076736 | tf_op jit(solution)/shard_map/convert_element_type | solution.py:171
  36.9 7.1 %all-to-all-start.2 = ((bf16[8,128,256]{2,1,0:T(8,128)(2,1)}), bf16[8,128,256]{2,1,0:T(8,128)(2,1)S(1)}, u32[]{:S(2)}, u32[]{:S(2)}) async-start(bf16[8,128,256]{2,1,0:T(8,128)(2,1)} %bitcast.4), calls=%async_computation.2 | async-start | bytes 1048576 | tf_op jit(solution)/shard_map/all_to_all | solution.py:172
  44.0 2.4 %scatter_custom_fusion.1 = s32[768]{0:T(1024)S(1)} fusion(s32[512]{0:T(512)S(1)} %bitcast.61, s32[512]{0:T(512)S(1)} %add_select_fusion, s32[]{:T(128)} %constant.38.clone.1), kind=kCustom, calls=%fused_computation.208 | custom fusion | bytes 3076 | tf_op jit(solution)/shard_map/scatter | solution.py:194
  46.5 0.1 copy.44
  46.6 0.1 copy.45
  46.8 6.6 %all-to-all-done.2 = bf16[8,128,256]{2,1,0:T(8,128)(2,1)S(1)} async-done(((bf16[8,128,256]{2,1,0:T(8,128)(2,1)}), bf16[8,128,256]{2,1,0:T(8,128)(2,1)S(1)}, u32[]{:S(2)}, u32[]{:S(2)}) %all-to-all-start.2) | async-done | bytes 524320 | tf_op jit(solution)/shard_map/all_to_all | solution.py:172
  53.4 1.0 copy.35
  54.4 1.5 convolution_bitcast_fusion
  55.9 0.3 copy.37
  56.3 0.3 fusion.44
  56.6 0.3 copy-done.7
  57.0 4.8 %multiply_reduce_fusion.1 = (f32[128]{0:T(128)S(1)}, f32[128,2048]{1,0:T(8,128)S(1)}) fusion(bf16[128,2048]{0,1:T(8,128)(2,1)S(1)} %fusion.44, bf16[2048,2048]{1,0:T(8,128)(2,1)} %param.17, bf16[128,2048]{1,0:T(8,128)(2,1)S(1)} %copy-done.7), kind=kOutput, calls=%fused_computation.99 | convolution fusion | flops 1075314560 | bytes 10486272 | tf_op jit(solution)/shard_map/dot_general | solution.py:181
  61.8 1.0 copy-done.3
  62.7 0.2 multiply_convert_fusion.1
  62.9 4.4 %gather_fusion = bf16[768,2048]{1,0:T(8,128)(2,1)} fusion(bf16[128,2048]{1,0:T(8,128)(2,1)S(1)} %multiply_convert_fusion.1, s32[1024]{0:T(1024)S(1)} %pad_clamp_fusion.1), kind=kCustom, calls=%fused_computation | custom fusion | bytes 6294528 | tf_op jit(solution)/shard_map/gather | solution.py:196
  67.3 4.2 %gather.9 = bf16[128,48,256]{2,1,0:T(8,128)(2,1)S(1)} reshape(bf16[768,2048]{1,0:T(8,128)(2,1)} %gather_fusion) | data formatting | bytes 6291456 | tf_op jit(solution)/shard_map/gather | solution.py:196
  71.5 1.1 broadcast_select_fusion.refs_0_
  72.7 43.7 %dispatch.1 = bf16[128,48,256]{2,1,0:T(8,128)(2,1)S(1)} custom-call(bf16[128,48,256]{2,1,0:T(8,128)(2,1)S(1)} %broadcast_select_fusion.refs_0_), custom_call_target="tpu_custom_call" | custom-call | tf_op jit(solution)/shard_map/dispatch/pallas_call | solution.py:117
  116.4 3.4 %reshape.198 = bf16[768,2048]{1,0:T(8,128)(2,1)} reshape(bf16[128,48,256]{2,1,0:T(8,128)(2,1)S(1)} %dispatch.1) | data formatting | bytes 6291456 | tf_op jit(solution)/shard_map/reshape | solution.py:199
  119.9 6.5 %fusion.2 = f32[768,1024]{1,0:T(8,128)S(1)} fusion(bf16[768,2048]{1,0:T(8,128)(2,1)} %reshape.198, bf16[1,2048,1024]{2,1,0:T(8,128)(2,1)} %param.22), kind=kOutput, calls=%fused_computation.6 | convolution fusion | flops 3221225472 | bytes 10485760 | tf_op jit(solution)/shard_map/dot_general | solution.py:56
  126.4 4.1 %multiply_convert_fusion = bf16[768,1024]{1,0:T(8,128)(2,1)S(1)} fusion(f32[768,1024]{1,0:T(8,128)S(1)} %fusion.2, bf16[768,2048]{1,0:T(8,128)(2,1)S(1)} %copy-done.5, bf16[1,2048,1024]{2,1,0:T(8,128)(2,1)S(1)} %copy-done.11), kind=kOutput, calls=%fused_computation.12 | convolution fusion | flops 3229089792 | bytes 12058624 | tf_op jit(solution)/shard_map/dot_general | solution.py:55
  130.6 4.8 %fusion.6 = bf16[768,2048]{1,0:T(8,128)(2,1)} fusion(bf16[768,1024]{1,0:T(8,128)(2,1)S(1)} %multiply_convert_fusion, bf16[1,1024,2048]{2,1,0:T(8,128)(2,1)S(1)} %copy-done.12), kind=kOutput, calls=%fused_computation.11 | convolution fusion | flops 3222798336 | bytes 8912896 | tf_op jit(solution)/shard_map/dot_general | solution.py:62
  135.4 4.2 %reshape.199.refs_0_ = bf16[128,48,256]{2,1,0:T(8,128)(2,1)S(1)} reshape(bf16[768,2048]{1,0:T(8,128)(2,1)} %fusion.6) | data formatting | bytes 6291456 | tf_op jit(solution)/shard_map/reshape | solution.py:204
  139.6 44.7 %giveback.1 = bf16[128,48,256]{2,1,0:T(8,128)(2,1)S(1)} custom-call(bf16[128,48,256]{2,1,0:T(8,128)(2,1)S(1)} %reshape.199.refs_0_), custom_call_target="tpu_custom_call" | custom-call | tf_op jit(solution)/shard_map/giveback/pallas_call | solution.py:117
  184.3 1.6 copy-done.2
  185.9 4.2 %reshape.200 = bf16[768,2048]{1,0:T(8,128)(2,1)S(1)} reshape(bf16[128,48,256]{2,1,0:T(8,128)(2,1)} %copy-done.2) | data formatting | bytes 6291456 | tf_op jit(solution)/shard_map/reshape | solution.py:205
  190.1 3.3 %gather_fusion.1 = bf16[512,2048]{1,0:T(8,128)(2,1)} fusion(bf16[768,2048]{1,0:T(8,128)(2,1)S(1)} %reshape.200, s32[1024]{0:T(1024)S(1)} %pad_clamp_fusion), kind=kCustom, calls=%fused_computation.1 | custom fusion | bytes 4196352 | tf_op jit(solution)/shard_map/gather | solution.py:205
  193.4 4.9 %reshape.201 = f32[128,4,2048]{2,1,0:T(4,128)} reshape(bf16[512,2048]{1,0:T(8,128)(2,1)} %gather_fusion.1) | data formatting | bytes 6291456 | tf_op jit(solution)/shard_map/convert_element_type | solution.py:206
  198.3 5.5 %multiply_reduce_fusion = f32[128,2048]{1,0:T(8,128)S(1)} fusion(f32[128,4,2048]{2,1,0:T(4,128)} %reshape.201, f32[128,4]{1,0:T(8,128)S(1)} %copy.45), kind=kLoop, calls=%fused_computation.10 | loop fusion | flops 1835008 | bytes 5244928 | tf_op jit(solution)/shard_map/reduce_sum | solution.py:207
  203.8 0.9 add_convert_fusion
  (71 shorter events, 1.4 us)
Async XLA Ops:
  0.0 54.4 %copy-start = (bf16[4,512,512]{2,1,0:T(8,128)(2,1)S(1)}, bf16[4,512,512]{2,1,0:T(8,128)(2,1)}, u32[]{:S(2)}) copy-start(bf16[4,512,512]{2,1,0:T(8,128)(2,1)} %param.15) | copy-start | bytes 6291460
  0.0 30.8 %copy-start.6 = (bf16[1024,256]{1,0:T(8,128)(2,1)S(1)}, bf16[1024,256]{1,0:T(8,128)(2,1)}, u32[]{:S(2)}) copy-start(bf16[1024,256]{1,0:T(8,128)(2,1)} %param.13) | copy-start | bytes 1572868
  0.0 46.6 %copy-start.10 = (f32[128,4]{0,1:T(4,128)S(1)}, f32[128,4]{0,1:T(4,128)}, u32[]{:S(2)}) copy-start(f32[128,4]{0,1:T(4,128)} %param.20) | copy-start | bytes 6148
  1.5 14.8 %all-to-all-start = ((s32[16,1,15]{2,1,0:T(1,128)}), s32[16,1,15]{2,1,0:T(1,128)S(1)}, u32[]{:S(2)}, u32[]{:S(2)}) async-start(s32[16,1,15]{2,1,0:T(1,128)} %broadcast_in_dim.162), calls=%async_computation | async-start | bytes 16384 | tf_op jit(solution)/shard_map/all_to_all | solution.py:19
  17.0 13.4 %all-to-all-start.1 = ((bf16[16,15,256]{2,1,0:T(8,128)(2,1)}), bf16[16,15,256]{2,1,0:T(8,128)(2,1)S(1)}, u32[]{:S(2)}, u32[]{:S(2)}) async-start(bf16[16,15,256]{2,1,0:T(8,128)(2,1)} %broadcast_in_dim.170), calls=%async_computation.1 | async-start | bytes 262144 | tf_op jit(solution)/shard_map/all_to_all | solution.py:19
  36.9 16.5 %all-to-all-start.2 = ((bf16[8,128,256]{2,1,0:T(8,128)(2,1)}), bf16[8,128,256]{2,1,0:T(8,128)(2,1)S(1)}, u32[]{:S(2)}, u32[]{:S(2)}) async-start(bf16[8,128,256]{2,1,0:T(8,128)(2,1)} %bitcast.4), calls=%async_computation.2 | async-start | bytes 1048576 | tf_op jit(solution)/shard_map/all_to_all | solution.py:172
  54.4 1.9 copy-start.8
  55.9 1.0 copy-start.7
  57.0 5.8 %copy-start.9 = (f32[2048]{0:T(1024)S(1)}, f32[2048]{0:T(1024)}, u32[]{:S(2)}) copy-start(f32[2048]{0:T(1024)} %param.18) | copy-start | bytes 24580
  61.7 1.0 copy-start.3
  119.9 6.5 %copy-start.5 = (bf16[768,2048]{1,0:T(8,128)(2,1)S(1)}, bf16[768,2048]{1,0:T(8,128)(2,1)}, u32[]{:S(2)}) copy-start(bf16[768,2048]{1,0:T(8,128)(2,1)} %reshape.198) | copy-start | bytes 9437188
  119.9 6.5 %copy-start.11 = (bf16[1,2048,1024]{2,1,0:T(8,128)(2,1)S(1)}, bf16[1,2048,1024]{2,1,0:T(8,128)(2,1)}, u32[]{:S(2)}) copy-start(bf16[1,2048,1024]{2,1,0:T(8,128)(2,1)} %param.21) | copy-start | bytes 12582916
  126.4 4.2 %copy-start.12 = (bf16[1,1024,2048]{2,1,0:T(8,128)(2,1)S(1)}, bf16[1,1024,2048]{2,1,0:T(8,128)(2,1)}, u32[]{:S(2)}) copy-start(bf16[1,1024,2048]{2,1,0:T(8,128)(2,1)} %param.23) | copy-start | bytes 12582916
  184.3 1.6 copy-start.2
  193.4 11.3 %copy-start.1 = (bf16[4,512,512]{2,1,0:T(8,128)(2,1)S(1)}, bf16[4,512,512]{2,1,0:T(8,128)(2,1)}, u32[]{:S(2)}) copy-start(bf16[4,512,512]{2,1,0:T(8,128)(2,1)} %param.15) | copy-start | bytes 6291460
  198.3 5.5 %copy-start.4 = (f32[128,2048]{1,0:T(8,128)S(1)}, f32[128,2048]{1,0:T(8,128)}, u32[]{:S(2)}) copy-start(f32[128,2048]{1,0:T(8,128)} %copy-done.3) | copy-start | bytes 3145732

commit v2 on v0

v2 whole, which is shorter than its diff:
```python
import functools

import jax
import jax.numpy as jnp
from jax import lax
from jax.experimental import pallas as pl
from jax.experimental.pallas import tpu as pltpu
from jax.sharding import PartitionSpec as P

GROUPS = 4
CAPACITY = 6
STRIDE = 37
INVERSE = 45
PARTS = 8
BATCH = 16
FIRST_WINDOW = 2

norm_eps = 1e-05
clamp_limit = 7.0
sigmoid_alpha = 1.702
MESH = pl.DeviceIdType.MESH
F32 = jnp.float32
BF16 = jnp.bfloat16


def iota(shape, axis):
    return lax.broadcasted_iota(jnp.int32, shape, axis)


def quotient(value, divisor):
    return jnp.floor((value.astype(F32) + 0.5) * (1.0 / divisor))


def dot(left, right):
    return jnp.dot(left, right, preferred_element_type=F32)


def layer_kernel(
    stream_hbm,
    projected_hbm,
    segments_hbm,
    group_hbm,
    scale_hbm,
    out_weight_hbm,
    gain_hbm,
    routes_hbm,
    weights_hbm,
    gate_hbm,
    up_hbm,
    down_hbm,
    combined_ref,
    stream_ref,
    extended,
    segments_ref,
    segments_before,
    group_ref,
    scale_ref,
    out_weight_ref,
    gain_ref,
    routes_ref,
    weights_ref,
    gate_ref,
    up_ref,
    down_ref,
    mixed_out,
    mixed_in,
    total,
    resid_ref,
    normed_ref,
    unpack_ref,
    pack_ref,
    rank_ref,
    rank_turned,
    share_turned,
    wide_ref,
    tall_ref,
    hidden_ref,
    sent,
    arrived,
    results,
    returned,
    load_sems,
    halo_sems,
    mixed_sends,
    mixed_recvs,
    sent_sem,
    arrived_sems,
    results_sem,
    returned_sems,
):
    sp_count, tp_count = lax.axis_size("sp"), lax.axis_size("tp")
    count = sp_count * tp_count
    sp, tp = lax.axis_index("sp"), lax.axis_index("tp")
    me = sp * tp_count + tp
    tokens, width = stream_ref.shape
    channels = width // tp_count
    group_width = width // GROUPS
    batches = count // BATCH
    rows = BATCH * CAPACITY
    piece = width // PARTS
    packed_rows = rows * PARTS
    message = CAPACITY * PARTS

    def device(index):
        return (index // tp_count, lax.rem(index, tp_count))

    loads = [
        pltpu.make_async_copy(source, target, load_sems.at[number])
        for number, (source, target) in enumerate(
            [
                (projected_hbm, extended.at[pl.ds(tokens, tokens * tp_count)]),
                (segments_hbm, segments_ref),
                (routes_hbm, routes_ref),
                (weights_hbm, weights_ref),
                (group_hbm, group_ref),
                (out_weight_hbm, out_weight_ref),
                (scale_hbm, scale_ref),
                (stream_hbm, stream_ref),
                (gain_hbm, gain_ref),
                (gate_hbm, gate_ref),
                (up_hbm, up_ref),
                (down_hbm, down_ref),
            ]
        )
    ]
    for load in loads:
        load.start()

    barrier = pltpu.get_barrier_semaphore()

    @pl.loop(1, count)
    def _(step):
        pl.semaphore_signal(
            barrier, inc=1, device_id=device(lax.rem(me + step, count)), device_id_type=MESH
        )

    window = jnp.left_shift(FIRST_WINDOW, tp // (tp_count // GROUPS))
    extended[pl.ds(0, tokens - 16), :] = jnp.zeros((tokens - 16, channels), BF16)
    for load in loads[:2]:
        load.wait()
    back = tokens + iota((tokens, 2 * tokens), 0) - iota((tokens, 2 * tokens), 1)
    in_window = (back >= 0) & (back < window)

    def pool(block, docs_before):
        docs = segments_ref[block : block + 1, :]
        docs_there = jnp.concatenate([docs_before, docs], axis=1).astype(F32)
        docs_here = jnp.broadcast_to(docs.astype(F32), (tokens, tokens)).T
        docs_here = jnp.concatenate([docs_here, docs_here], axis=1)
        included = jnp.where(in_window & (docs_here == docs_there), 1.0, 0.0).astype(BF16)
        sums = dot(included, extended[pl.ds(block * tokens, 2 * tokens), :])
        counts = dot(included, jnp.ones((2 * tokens, channels), BF16))
        own = extended[pl.ds((block + 1) * tokens, tokens), :].astype(F32)
        mixed_out[block] = (sums / counts - own).astype(BF16)

    for block in range(1, tp_count):
        pool(block, segments_ref[block - 1 : block, :])

    for load in loads[2:4]:
        load.wait()
    order = jnp.bitwise_and((routes_ref[...] - me) * INVERSE, count - 1)
    square = (count, tokens)
    chosen = jnp.zeros(square, F32)
    share = jnp.zeros(square, F32)
    for choice in range(routes_ref.shape[0]):
        match = iota(square, 0) == order[choice : choice + 1, :]
        chosen = chosen + jnp.where(match, 1.0, 0.0)
        share = share + jnp.where(match, weights_ref[choice : choice + 1, :], 0.0)
    earlier = jnp.where(iota((tokens, tokens), 0) < iota((tokens, tokens), 1), 1.0, 0.0)
    rank = jnp.where(chosen > 0.0, dot(chosen.astype(BF16), earlier.astype(BF16)), -1.0)
    rank_ref[...] = rank.astype(BF16)
    rank_turned[...] = rank.T.astype(BF16)
    share = share.T
    share_high = share.astype(BF16)
    share_turned[0] = share_high
    share_turned[1] = (share - share_high.astype(F32)).astype(BF16)

    turned = (packed_rows, packed_rows)

    def message_row(value):
        part = quotient(value, rows)
        within = value.astype(F32) - part * rows
        peer = quotient(within, CAPACITY)
        return peer * message + part * CAPACITY + (within - peer * CAPACITY)

    unpack_ref[...] = jnp.where(
        message_row(iota((packed_rows, 1), 0)) == iota(turned, 1).astype(F32), 1.0, 0.0
    ).astype(BF16)
    pack_ref[...] = jnp.where(
        message_row(iota((1, packed_rows), 1)) == iota(turned, 0).astype(F32), 1.0, 0.0
    ).astype(BF16)

    def packed():
        return dot(pack_ref[...], tall_ref[...]).astype(BF16).reshape(BATCH, message, piece)

    def unpack(block):
        tall = dot(unpack_ref[...], block.reshape(packed_rows, piece)).astype(BF16)
        for part in range(PARTS):
            wide_ref[:, part * piece : (part + 1) * piece] = tall[part * rows : (part + 1) * rows]

    pl.semaphore_wait(barrier, count - 1)

    following = (lax.rem(sp + 1, sp_count), tp)
    halo = [
        pltpu.make_async_remote_copy(
            extended.at[pl.ds(tokens * (tp_count + 1) - 16, 16)],
            extended.at[pl.ds(tokens - 16, 16)],
            halo_sems.at[0],
            halo_sems.at[1],
            device_id=following,
            device_id_type=MESH,
        ),
        pltpu.make_async_remote_copy(
            segments_ref,
            segments_before,
            halo_sems.at[2],
            halo_sems.at[3],
            device_id=following,
            device_id_type=MESH,
        ),
    ]
    for copy in halo:
        copy.start()

    def mixed_copy(peer):
        return pltpu.make_async_remote_copy(
            mixed_out.at[peer],
            mixed_in.at[tp],
            mixed_sends.at[peer],
            mixed_recvs.at[tp],
            device_id=(sp, peer),
            device_id_type=MESH,
        )

    for step in range(1, tp_count):
        peer = lax.rem(tp + step, tp_count)

        @pl.when(peer != 0)
        def _():
            mixed_copy(peer).start()

    for copy in halo:
        copy.wait()
    docs_before = jnp.where(sp > 0, segments_before[tp_count - 1 : tp_count, :], -1)
    pool(0, docs_before)

    @pl.when(tp != 0)
    def _():
        mixed_copy(0).start()

    mixed_in[tp] = mixed_out[tp]

    for load in loads[4:9]:
        load.wait()
    total[...] = stream_ref[...].astype(F32)
    for step in (0, 1, 3, 2):
        per_group = tp_count // GROUPS
        group = lax.rem(tp // per_group + step, GROUPS)
        grouped = jnp.zeros((tokens, group_width), F32)
        for member in range(per_group):
            source = group * per_group + member

            @pl.when(source != tp)
            def _():
                block = mixed_in.at[source]
                pltpu.make_async_copy(block, block, mixed_recvs.at[source]).wait()

            grouped = grouped + dot(
                mixed_in[source], group_ref[group, member * channels : (member + 1) * channels, :]
            )
        scale = scale_ref[:, pl.ds(pl.multiple_of(group * group_width, group_width), group_width)]
        total[...] += dot((grouped * scale).astype(BF16), out_weight_ref[group])

    resid = total[...].astype(BF16)
    resid_ref[...] = resid
    values = resid.astype(F32)
    inverse = lax.rsqrt(jnp.mean(values * values, -1, keepdims=True) + norm_eps)
    normed_ref[...] = (values * inverse * gain_ref[...]).astype(BF16)

    @pl.loop(0, batches)
    def _(batch):
        names = (batch * BATCH).astype(F32) + quotient(iota((rows, count), 0), CAPACITY)
        slot = iota((rows, 1), 0).astype(F32) - CAPACITY * quotient(iota((rows, 1), 0), CAPACITY)
        spread = jnp.where(names == iota((rows, count), 1).astype(F32), 1.0, 0.0).astype(BF16)
        select = jnp.where(dot(spread, rank_ref[...]) == slot, 1.0, 0.0).astype(BF16)
        for part in range(PARTS):
            tall_ref[part * rows : (part + 1) * rows, :] = dot(
                select, normed_ref[:, part * piece : (part + 1) * piece]
            ).astype(BF16)
        sent[pl.ds(batch * BATCH, BATCH)] = packed()

        @pl.when(batch == 0)
        def _():
            arrived[0] = sent[0]

        @pl.loop(jnp.where(batch == 0, 1, 0), BATCH)
        def _(step):
            name = batch * BATCH + step
            pltpu.make_async_remote_copy(
                sent.at[name],
                arrived.at[name],
                sent_sem,
                arrived_sems.at[batch],
                device_id=device(lax.rem(me + name * STRIDE, count)),
                device_id_type=MESH,
            ).start()

    def wait_batch(buffer, sems, batch):
        @pl.when(batch == 0)
        def _():
            part = buffer.at[pl.ds(1, BATCH - 1)]
            pltpu.make_async_copy(part, part, sems.at[0]).wait()

        @pl.when(batch != 0)
        def _():
            part = buffer.at[pl.ds(batch * BATCH, BATCH)]
            pltpu.make_async_copy(part, part, sems.at[batch]).wait()

    for load in loads[9:]:
        load.wait()

    @pl.loop(0, batches)
    def _(batch):
        wait_batch(arrived, arrived_sems, batch)
        unpack(arrived[pl.ds(batch * BATCH, BATCH)])
        block = wide_ref[...]
        hidden = hidden_ref.shape[1]
        for start in range(0, hidden, 256):
            columns = slice(start, start + 256)
            gated = jnp.minimum(dot(block, gate_ref[0, :, columns]), clamp_limit)
            linear = jnp.clip(dot(block, up_ref[0, :, columns]), -clamp_limit, clamp_limit)
            hidden_ref[:, columns] = (
                gated * jax.nn.sigmoid(sigmoid_alpha * gated) * (linear + 1.0)
            ).astype(BF16)
        for part in range(PARTS):
            tall_ref[part * rows : (part + 1) * rows, :] = dot(
                hidden_ref[...], down_ref[0, :, part * piece : (part + 1) * piece]
            ).astype(BF16)
        results[pl.ds(batch * BATCH, BATCH)] = packed()

        @pl.when(batch == 0)
        def _():
            returned[0] = results[0]

        @pl.loop(jnp.where(batch == 0, 1, 0), BATCH)
        def _(step):
            name = batch * BATCH + step
            pltpu.make_async_remote_copy(
                results.at[name],
                returned.at[name],
                results_sem,
                returned_sems.at[batch],
                device_id=device(lax.rem(me + (count - name) * STRIDE, count)),
                device_id_type=MESH,
            ).start()

    total[...] = resid_ref[...].astype(F32)

    @pl.loop(0, batches)
    def _(batch):
        names = (batch * BATCH).astype(F32) + quotient(iota((count, rows), 1), CAPACITY)
        slot = iota((1, rows), 1).astype(F32) - CAPACITY * quotient(iota((1, rows), 1), CAPACITY)
        spread = jnp.where(names == iota((count, rows), 0).astype(F32), 1.0, 0.0).astype(BF16)
        live = dot(rank_turned[...], spread) == slot
        high = jnp.where(live, dot(share_turned[0], spread), 0.0).astype(BF16)
        low = jnp.where(live, dot(share_turned[1], spread), 0.0).astype(BF16)
        wait_batch(returned, returned_sems, batch)
        unpack(returned[pl.ds(batch * BATCH, BATCH)])
        total[...] += dot(high, wide_ref[...]) + dot(low, wide_ref[...])

    combined_ref[...] = total[...].astype(BF16)

    for step in range(1, tp_count):
        mixed_copy(lax.rem(tp + step, tp_count)).wait_send()
    rest = pl.ds(1, count - 1)
    pltpu.make_async_copy(sent.at[rest], sent.at[rest], sent_sem).wait()
    pltpu.make_async_copy(results.at[rest], results.at[rest], results_sem).wait()


def body(
    stream,
    projected,
    segments,
    group_weight,
    group_scale,
    out_weight,
    ffn_gain,
    routes,
    route_weights,
    expert_gate,
    expert_up,
    expert_down,
):
    tokens, width = stream.shape
    tp_count = lax.axis_size("tp")
    count = lax.axis_size("sp") * tp_count
    channels = width // tp_count
    hidden = expert_gate.shape[2]
    rows = BATCH * CAPACITY
    piece = width // PARTS
    operands = (
        stream,
        projected,
        segments.reshape(-1, tokens),
        group_weight,
        group_scale.reshape(1, -1),
        out_weight.reshape(GROUPS, width // GROUPS, width),
        ffn_gain.reshape(1, -1),
        routes.T,
        route_weights.T,
        expert_gate,
        expert_up,
        expert_down,
    )
    messages = (count, CAPACITY * PARTS, piece)
    batches = count // BATCH
    vmem = pltpu.VMEM
    dma = pltpu.SemaphoreType.DMA
    return pl.pallas_call(
        layer_kernel,
        out_shape=jax.ShapeDtypeStruct((tokens, width), BF16),
        in_specs=[pl.BlockSpec(memory_space=pl.ANY)] * len(operands),
        out_specs=pl.BlockSpec(memory_space=pltpu.VMEM),
        scratch_shapes=[
            vmem((tokens, width), BF16),
            vmem((tokens * (tp_count + 1), channels), BF16),
            vmem((tp_count, tokens), jnp.int32),
            vmem((tp_count, tokens), jnp.int32),
            vmem(group_weight.shape, BF16),
            vmem((1, width), F32),
            vmem((GROUPS, width // GROUPS, width), BF16),
            vmem((1, width), F32),
            vmem(routes.shape[::-1], jnp.int32),
            vmem(routes.shape[::-1], F32),
            vmem(expert_gate.shape, BF16),
            vmem(expert_up.shape, BF16),
            vmem(expert_down.shape, BF16),
            vmem((tp_count, tokens, channels), BF16),
            vmem((tp_count, tokens, channels), BF16),
            vmem((tokens, width), F32),
            vmem((tokens, width), BF16),
            vmem((tokens, width), BF16),
            vmem((rows * PARTS, rows * PARTS), BF16),
            vmem((rows * PARTS, rows * PARTS), BF16),
            vmem((count, tokens), BF16),
            vmem((tokens, count), BF16),
            vmem((2, tokens, count), BF16),
            vmem((rows, width), BF16),
            vmem((rows * PARTS, piece), BF16),
            vmem((rows, hidden), BF16),
            vmem(messages, BF16),
            vmem(messages, BF16),
            vmem(messages, BF16),
            vmem(messages, BF16),
            dma((len(operands),)),
            dma((4,)),
            dma((tp_count,)),
            dma((tp_count,)),
            dma,
            dma((batches,)),
            dma,
            dma((batches,)),
        ],
        name="layer",
        compiler_params=pltpu.CompilerParams(
            collective_id=0, has_side_effects=True, vmem_limit_bytes=60 << 20
        ),
    )(*operands)


def solution(mesh):
    in_specs = (
        P(("sp", "tp"), None),
        P("sp", "tp"),
        P("sp"),
        P(),
        P(),
        P(),
        P(),
        P(("sp", "tp"), None),
        P(("sp", "tp"), None),
        P(("sp", "tp"), None, None),
        P(("sp", "tp"), None, None),
        P(("sp", "tp"), None, None),
    )
    out_specs = P(("sp", "tp"), None)
    return jax.shard_map(body, mesh=mesh, in_specs=in_specs, out_specs=out_specs, check_vma=False)
```

time: 231 us -> 99.6 us (0.43)
  Pallas kernels: 0 us -> 96.3 us
  waiting for transfers between devices: 64.2 us -> 0 us
  blocking collectives: 57.7 us -> 0 us
  local copies, waits for them, and re-layouts: 43.6 us -> 1.88 us
  starting transfers between devices: 25.2 us -> 0 us
  other arithmetic: 19.7 us -> 0 us
  matrix products: 19.4 us -> 0 us
    pallas_call x0 -> x1, Pallas kernels: none -> 96.3 us  [body(): pl.pallas_call(layer_kernel, out_shape=jax.ShapeDtypeStruct((tokens, widt...]
    all_to_all x4 -> x0, waiting for transfers between devices: 64.2 us -> none  [the longest x1 52.7 us: body(): lax.all_to_all(results, ('sp', 'tp'), split_axis=0, concat_axis=0, tiled=...]
    all_to_all x1 -> x0, blocking collectives: 57.7 us -> none  [body(): lax.all_to_all(outgoing.reshape(expert_count, capacity, model_width), ('s...]
    all_to_all x4 -> x0, starting transfers between devices: 25.2 us -> none  [the longest x2 12.2 us: sent_to_all(): lax.all_to_all(jnp.broadcast_to(value[None], (devices, *value.shape)), ax...]
    dot_general x5 -> x0, matrix products: 19.4 us -> none  [the longest x1 5.35 us: run_expert(): up_value = jnp.dot(flat_rows, up_matrix, preferred_element_type=jnp.float32)]
    gather x3 -> x0, local copies, waits for them, and re-layouts: 13.8 us -> none  [the longest x2 10.5 us: body(): normed[slot_token]]
    reshape x3 -> x0, local copies, waits for them, and re-layouts: 12.6 us -> none  [the longest x1 4.87 us: run_expert(): flat_rows = block.reshape(-1, block.shape[-1])]
    convert_element_type x5 -> x0, other arithmetic: 7.56 us -> none  [the longest x1 6.15 us: body(): (window_sum / window_count - projected.astype(jnp.float32)).astype(jnp.bf...]
  transfers between devices with their start and end apart: 4 -> 0, of which waited for: 4 -> 0; matrix products, arithmetic and copies ran while one was open for 5% -> 0% of each run, Pallas kernels for 0% -> 0%
where the time goes in v2:
time: 99.6 us; the launch traced here: 98.1 us
  Pallas kernels  96.3 us (97%)
  local copies, waits for them, and re-layouts  1.88 us (2%)
    pallas_call x1, Pallas kernels, body(): pl.pallas_call(layer_kernel, out_shape=jax.ShapeDtypeStruct((tokens, widt...  96.3 us

profile of v2, /device:TPU:1, one launch (start us, length us, event | category | flops | bytes accessed | tf_op | source)
XLA Modules:
  0.0 98.1 jit_solution(2438072929407032629)
XLA Ops:
  0.0 96.3 %layer.1 = bf16[128,2048]{1,0:T(8,128)(2,1)} custom-call(bf16[128,2048]{1,0:T(8,128)(2,1)} %stream_hbm.1, bf16[1024,256]{1,0:T(8,128)(2,1)} %projected_hbm.1, s32[8,128]{1,0:T(8,128)} %bitcast.9, bf16[4,512,512]{2,1,0:T(8,128)(2,1)} %group_hbm.1, f32[1,2048]{1,0:T(1,128)} %bitcast.7, bf16[4,512,2048]{2,1,0:T(8,128)(2,1)} %bitcast.6, f32[1,2048]{1,0:T(1,128)} %bitcast.8, ...), custom_call_target="tpu_custom_call" | custom-call | tf_op jit(solution)/shard_map/layer/pallas_call | solution.py:418
  96.3 1.9 %copy.14 = bf16[128,2048]{1,0:T(8,128)(2,1)} copy(bf16[128,2048]{1,0:T(8,128)(2,1)} %layer.1) | data formatting | bytes 1048576

commit v3 on v2

--- a/solution.py
+++ b/solution.py
@@ -72,6 +72,7 @@
     rank_ref,
     rank_turned,
     share_turned,
+    picks,
     wide_ref,
     tall_ref,
     hidden_ref,
@@ -87,6 +88,7 @@
     arrived_sems,
     results_sem,
     returned_sems,
+    ready,
 ):
     sp_count, tp_count = lax.axis_size("sp"), lax.axis_size("tp")
     count = sp_count * tp_count
@@ -128,11 +130,35 @@
 
     barrier = pltpu.get_barrier_semaphore()
 
-    @pl.loop(1, count)
-    def _(step):
+    for step in range(1, tp_count):
         pl.semaphore_signal(
-            barrier, inc=1, device_id=device(lax.rem(me + step, count)), device_id_type=MESH
+            barrier,
+            inc=1,
+            device_id=(sp, lax.rem(tp + step, tp_count)),
+            device_id_type=MESH,
         )
+    for step in range(1, sp_count):
+        pl.semaphore_signal(
+            barrier,
+            inc=1,
+            device_id=(lax.rem(sp + step, sp_count), tp),
+            device_id_type=MESH,
+        )
+
+    turned = (packed_rows, packed_rows)
+
+    def message_row(value):
+        part = quotient(value, rows)
+        within = value.astype(F32) - part * rows
+        peer = quotient(within, CAPACITY)
+        return peer * message + part * CAPACITY + (within - peer * CAPACITY)
+
+    unpack_ref[...] = jnp.where(
+        message_row(iota((packed_rows, 1), 0)) == iota(turned, 1).astype(F32), 1.0, 0.0
+    ).astype(BF16)
+    pack_ref[...] = jnp.where(
+        message_row(iota((1, packed_rows), 1)) == iota(turned, 0).astype(F32), 1.0, 0.0
+    ).astype(BF16)
 
     window = jnp.left_shift(FIRST_WINDOW, tp // (tp_count // GROUPS))
     extended[pl.ds(0, tokens - 16), :] = jnp.zeros((tokens - 16, channels), BF16)
@@ -155,49 +181,7 @@
     for block in range(1, tp_count):
         pool(block, segments_ref[block - 1 : block, :])
 
-    for load in loads[2:4]:
-        load.wait()
-    order = jnp.bitwise_and((routes_ref[...] - me) * INVERSE, count - 1)
-    square = (count, tokens)
-    chosen = jnp.zeros(square, F32)
-    share = jnp.zeros(square, F32)
-    for choice in range(routes_ref.shape[0]):
-        match = iota(square, 0) == order[choice : choice + 1, :]
-        chosen = chosen + jnp.where(match, 1.0, 0.0)
-        share = share + jnp.where(match, weights_ref[choice : choice + 1, :], 0.0)
-    earlier = jnp.where(iota((tokens, tokens), 0) < iota((tokens, tokens), 1), 1.0, 0.0)
-    rank = jnp.where(chosen > 0.0, dot(chosen.astype(BF16), earlier.astype(BF16)), -1.0)
-    rank_ref[...] = rank.astype(BF16)
-    rank_turned[...] = rank.T.astype(BF16)
-    share = share.T
-    share_high = share.astype(BF16)
-    share_turned[0] = share_high
-    share_turned[1] = (share - share_high.astype(F32)).astype(BF16)
-
-    turned = (packed_rows, packed_rows)
-
-    def message_row(value):
-        part = quotient(value, rows)
-        within = value.astype(F32) - part * rows
-        peer = quotient(within, CAPACITY)
-        return peer * message + part * CAPACITY + (within - peer * CAPACITY)
-
-    unpack_ref[...] = jnp.where(
-        message_row(iota((packed_rows, 1), 0)) == iota(turned, 1).astype(F32), 1.0, 0.0
-    ).astype(BF16)
-    pack_ref[...] = jnp.where(
-        message_row(iota((1, packed_rows), 1)) == iota(turned, 0).astype(F32), 1.0, 0.0
-    ).astype(BF16)
-
-    def packed():
-        return dot(pack_ref[...], tall_ref[...]).astype(BF16).reshape(BATCH, message, piece)
-
-    def unpack(block):
-        tall = dot(unpack_ref[...], block.reshape(packed_rows, piece)).astype(BF16)
-        for part in range(PARTS):
-            wide_ref[:, part * piece : (part + 1) * piece] = tall[part * rows : (part + 1) * rows]
-
-    pl.semaphore_wait(barrier, count - 1)
+    pl.semaphore_wait(barrier, sp_count + tp_count - 2)
 
     following = (lax.rem(sp + 1, sp_count), tp)
     halo = [
@@ -238,6 +222,46 @@
         def _():
             mixed_copy(peer).start()
 
+    for step in range(1, sp_count):
+        pl.semaphore_signal(
+            ready, inc=1, device_id=(lax.rem(sp + step, sp_count), tp), device_id_type=MESH
+        )
+
+    def packed():
+        return dot(pack_ref[...], tall_ref[...]).astype(BF16).reshape(BATCH, message, piece)
+
+    def unpack(block):
+        tall = dot(unpack_ref[...], block.reshape(packed_rows, piece)).astype(BF16)
+        for part in range(PARTS):
+            wide_ref[:, part * piece : (part + 1) * piece] = tall[part * rows : (part + 1) * rows]
+
+    for load in loads[2:4]:
+        load.wait()
+    order = jnp.bitwise_and((routes_ref[...] - me) * INVERSE, count - 1)
+    square = (count, tokens)
+    chosen = jnp.zeros(square, F32)
+    share = jnp.zeros(square, F32)
+    for choice in range(routes_ref.shape[0]):
+        match = iota(square, 0) == order[choice : choice + 1, :]
+        chosen = chosen + jnp.where(match, 1.0, 0.0)
+        share = share + jnp.where(match, weights_ref[choice : choice + 1, :], 0.0)
+    earlier = jnp.where(iota((tokens, tokens), 0) < iota((tokens, tokens), 1), 1.0, 0.0)
+    rank = jnp.where(chosen > 0.0, dot(chosen.astype(BF16), earlier.astype(BF16)), -1.0)
+    rank_ref[...] = rank.astype(BF16)
+    rank_turned[...] = rank.T.astype(BF16)
+
+    @pl.loop(0, batches)
+    def _(batch):
+        names = (batch * BATCH).astype(F32) + quotient(iota((rows, count), 0), CAPACITY)
+        slot = iota((rows, 1), 0).astype(F32) - CAPACITY * quotient(iota((rows, 1), 0), CAPACITY)
+        spread = jnp.where(names == iota((rows, count), 1).astype(F32), 1.0, 0.0).astype(BF16)
+        picks[batch] = jnp.where(dot(spread, rank_ref[...]) == slot, 1.0, 0.0).astype(BF16)
+
+    share = share.T
+    share_high = share.astype(BF16)
+    share_turned[0] = share_high
+    share_turned[1] = (share - share_high.astype(F32)).astype(BF16)
+
     for copy in halo:
         copy.wait()
     docs_before = jnp.where(sp > 0, segments_before[tp_count - 1 : tp_count, :], -1)
@@ -276,12 +300,11 @@
     inverse = lax.rsqrt(jnp.mean(values * values, -1, keepdims=True) + norm_eps)
     normed_ref[...] = (values * inverse * gain_ref[...]).astype(BF16)
 
+    pl.semaphore_wait(ready, sp_count - 1)
+
     @pl.loop(0, batches)
     def _(batch):
-        names = (batch * BATCH).astype(F32) + quotient(iota((rows, count), 0), CAPACITY)
-        slot = iota((rows, 1), 0).astype(F32) - CAPACITY * quotient(iota((rows, 1), 0), CAPACITY)
-        spread = jnp.where(names == iota((rows, count), 1).astype(F32), 1.0, 0.0).astype(BF16)
-        select = jnp.where(dot(spread, rank_ref[...]) == slot, 1.0, 0.0).astype(BF16)
+        select = picks[batch]
         for part in range(PARTS):
             tall_ref[part * rows : (part + 1) * rows, :] = dot(
                 select, normed_ref[:, part * piece : (part + 1) * piece]
@@ -418,7 +441,7 @@
     return pl.pallas_call(
         layer_kernel,
         out_shape=jax.ShapeDtypeStruct((tokens, width), BF16),
-        in_specs=[pl.BlockSpec(memory_space=pl.ANY)] * len(operands),
+        in_specs=[pl.BlockSpec(memory_space=pltpu.MemorySpace.HBM)] * len(operands),
         out_specs=pl.BlockSpec(memory_space=pltpu.VMEM),
         scratch_shapes=[
             vmem((tokens, width), BF16),
@@ -444,6 +467,7 @@
             vmem((count, tokens), BF16),
             vmem((tokens, count), BF16),
             vmem((2, tokens, count), BF16),
+            vmem((batches, rows, tokens), BF16),
             vmem((rows, width), BF16),
             vmem((rows * PARTS, piece), BF16),
             vmem((rows, hidden), BF16),
@@ -459,12 +483,13 @@
             dma((batches,)),
             dma,
             dma((batches,)),
+            pltpu.SemaphoreType.REGULAR,
         ],
         name="layer",
         compiler_params=pltpu.CompilerParams(
-            collective_id=0, has_side_effects=True, vmem_limit_bytes=60 << 20
+            collective_id=0, has_side_effects=True, vmem_limit_bytes=50 << 20
         ),
-    )(*operands)
+    )(*(pltpu.with_memory_space_constraint(operand, pltpu.MemorySpace.HBM) for operand in operands))
 
 
 def solution(mesh):

time: 99.6 us -> 93.3 us (0.937)
  Pallas kernels: 96.3 us -> 92 us
  local copies, waits for them, and re-layouts: 1.88 us -> 0.8 us
    pallas_call x1, Pallas kernels: 96.3 us -> 92 us  [body(): pl.pallas_call(layer_kernel, out_shape=jax.ShapeDtypeStruct((tokens, widt...]
    unnamed x1, local copies, waits for them, and re-layouts: 1.88 us -> 0.8 us
where the time goes in v3:
time: 93.3 us; the launch traced here: 92.8 us
  Pallas kernels  92 us (99%)
    pallas_call x1, Pallas kernels, body(): pl.pallas_call(layer_kernel, out_shape=jax.ShapeDtypeStruct((tokens, widt...  92 us

profile of v3, /device:TPU:1, one launch (start us, length us, event | category | flops | bytes accessed | tf_op | source)
XLA Modules:
  0.0 92.8 jit_solution(7526687634455625923)
XLA Ops:
  0.0 92.0 %layer.1 = bf16[128,2048]{1,0:T(8,128)(2,1)S(1)} custom-call(bf16[128,2048]{1,0:T(8,128)(2,1)} %stream_hbm.1, bf16[1024,256]{1,0:T(8,128)(2,1)} %projected_hbm.1, s32[8,128]{1,0:T(8,128)} %bitcast.9, bf16[4,512,512]{2,1,0:T(8,128)(2,1)} %group_hbm.1, f32[1,2048]{1,0:T(1,128)} %bitcast.7, bf16[4,512,2048]{2,1,0:T(8,128)(2,1)} %bitcast.6, f32[1,2048]{1,0:T(1,128)} %bitcast.8, ...), custom_call_target="tpu_custom_call" | custom-call | tf_op jit(solution)/shard_map/layer/pallas_call | solution.py:441
  92.0 0.8 copy.14

commit v4 on v3

--- a/solution.py
+++ b/solution.py
@@ -9,8 +9,9 @@
 
 GROUPS = 4
 CAPACITY = 6
-STRIDE = 37
-INVERSE = 45
+STRIDE = 101
+INVERSE = 109
+RING = 4
 PARTS = 8
 BATCH = 16
 FIRST_WINDOW = 2
@@ -93,7 +94,6 @@
     sp_count, tp_count = lax.axis_size("sp"), lax.axis_size("tp")
     count = sp_count * tp_count
     sp, tp = lax.axis_index("sp"), lax.axis_index("tp")
-    me = sp * tp_count + tp
     tokens, width = stream_ref.shape
     channels = width // tp_count
     group_width = width // GROUPS
@@ -103,8 +103,19 @@
     packed_rows = rows * PARTS
     message = CAPACITY * PARTS
 
-    def device(index):
-        return (index // tp_count, lax.rem(index, tp_count))
+    def peer_at(name, sign):
+        step = lax.rem(name * STRIDE, count)
+        sender = lax.rem(tp, 2) if sign > 0 else lax.rem(tp + step, 2)
+        way = sign * (1 - 2 * sender)
+        place = [
+            lax.rem(index + way * part + RING, RING)
+            for index, part in (
+                (sp // RING, step // (2 * RING * RING)),
+                (lax.rem(sp, RING), lax.rem(step // (2 * RING), RING)),
+                (tp // 2, lax.rem(step // 2, RING)),
+            )
+        ]
+        return (place[0] * RING + place[1], place[2] * 2 + lax.rem(tp + step, 2))
 
     loads = [
         pltpu.make_async_copy(source, target, load_sems.at[number])
@@ -237,7 +248,13 @@
 
     for load in loads[2:4]:
         load.wait()
-    order = jnp.bitwise_and((routes_ref[...] - me) * INVERSE, count - 1)
+    named = routes_ref[...]
+    offset = jnp.bitwise_and(named + tp, 1)
+    way = 1 - 2 * lax.rem(tp, 2)
+    for unit, own in ((2, tp // 2), (2 * RING, lax.rem(sp, RING)), (2 * RING * RING, sp // RING)):
+        place = lax.shift_right_logical(named, unit.bit_length() - 1)
+        offset = offset + jnp.bitwise_and((place - own) * way, RING - 1) * unit
+    order = jnp.bitwise_and(offset * INVERSE, count - 1)
     square = (count, tokens)
     chosen = jnp.zeros(square, F32)
     share = jnp.zeros(square, F32)
@@ -323,7 +340,7 @@
                 arrived.at[name],
                 sent_sem,
                 arrived_sems.at[batch],
-                device_id=device(lax.rem(me + name * STRIDE, count)),
+                device_id=peer_at(name, 1),
                 device_id_type=MESH,
             ).start()
 
@@ -372,7 +389,7 @@
                 returned.at[name],
                 results_sem,
                 returned_sems.at[batch],
-                device_id=device(lax.rem(me + (count - name) * STRIDE, count)),
+                device_id=peer_at(name, -1),
                 device_id_type=MESH,
             ).start()
 

time: 93.3 us -> 91.4 us (0.980)
  Pallas kernels: 92 us -> 90.5 us
    pallas_call x1, Pallas kernels: 92 us -> 90.5 us  [body(): pl.pallas_call(layer_kernel, out_shape=jax.ShapeDtypeStruct((tokens, widt...]
where the time goes in v4:
time: 91.4 us; the launch traced here: 91.3 us
  Pallas kernels  90.5 us (99%)
    pallas_call x1, Pallas kernels, body(): pl.pallas_call(layer_kernel, out_shape=jax.ShapeDtypeStruct((tokens, widt...  90.5 us

profile of v4, /device:TPU:1, one launch (start us, length us, event | category | flops | bytes accessed | tf_op | source)
XLA Modules:
  0.0 91.3 jit_solution(17731965973779175211)
XLA Ops:
  0.0 90.5 %layer.1 = bf16[128,2048]{1,0:T(8,128)(2,1)S(1)} custom-call(bf16[128,2048]{1,0:T(8,128)(2,1)} %stream_hbm.1, bf16[1024,256]{1,0:T(8,128)(2,1)} %projected_hbm.1, s32[8,128]{1,0:T(8,128)} %bitcast.9, bf16[4,512,512]{2,1,0:T(8,128)(2,1)} %group_hbm.1, f32[1,2048]{1,0:T(1,128)} %bitcast.7, bf16[4,512,2048]{2,1,0:T(8,128)(2,1)} %bitcast.6, f32[1,2048]{1,0:T(1,128)} %bitcast.8, ...), custom_call_target="tpu_custom_call" | custom-call | tf_op jit(solution)/shard_map/layer/pallas_call | solution.py:458
  90.5 0.8 copy.14

commit v5 on v4

--- a/solution.py
+++ b/solution.py
@@ -238,8 +238,9 @@
             ready, inc=1, device_id=(lax.rem(sp + step, sp_count), tp), device_id_type=MESH
         )
 
-    def packed():
-        return dot(pack_ref[...], tall_ref[...]).astype(BF16).reshape(BATCH, message, piece)
+    def packed(half):
+        chosen_rows = pack_ref[half * packed_rows // 2 : (half + 1) * packed_rows // 2, :]
+        return dot(chosen_rows, tall_ref[...]).astype(BF16).reshape(BATCH // 2, message, piece)
 
     def unpack(block):
         tall = dot(unpack_ref[...], block.reshape(packed_rows, piece)).astype(BF16)
@@ -326,23 +327,26 @@
             tall_ref[part * rows : (part + 1) * rows, :] = dot(
                 select, normed_ref[:, part * piece : (part + 1) * piece]
             ).astype(BF16)
-        sent[pl.ds(batch * BATCH, BATCH)] = packed()
-
-        @pl.when(batch == 0)
-        def _():
-            arrived[0] = sent[0]
-
-        @pl.loop(jnp.where(batch == 0, 1, 0), BATCH)
-        def _(step):
-            name = batch * BATCH + step
-            pltpu.make_async_remote_copy(
-                sent.at[name],
-                arrived.at[name],
-                sent_sem,
-                arrived_sems.at[batch],
-                device_id=peer_at(name, 1),
-                device_id_type=MESH,
-            ).start()
+        for half in range(2):
+            sent[pl.ds(batch * BATCH + half * BATCH // 2, BATCH // 2)] = packed(half)
+
+            if half == 0:
+
+                @pl.when(batch == 0)
+                def _():
+                    arrived[0] = sent[0]
+
+            @pl.loop(jnp.where(batch == 0, 1 - half, 0), BATCH // 2)
+            def _(step):
+                name = batch * BATCH + half * BATCH // 2 + step
+                pltpu.make_async_remote_copy(
+                    sent.at[name],
+                    arrived.at[name],
+                    sent_sem,
+                    arrived_sems.at[batch],
+                    device_id=peer_at(name, 1),
+                    device_id_type=MESH,
+                ).start()
 
     def wait_batch(buffer, sems, batch):
         @pl.when(batch == 0)
@@ -375,23 +379,26 @@
             tall_ref[part * rows : (part + 1) * rows, :] = dot(
                 hidden_ref[...], down_ref[0, :, part * piece : (part + 1) * piece]
             ).astype(BF16)
-        results[pl.ds(batch * BATCH, BATCH)] = packed()
-
-        @pl.when(batch == 0)
-        def _():
-            returned[0] = results[0]
-
-        @pl.loop(jnp.where(batch == 0, 1, 0), BATCH)
-        def _(step):
-            name = batch * BATCH + step
-            pltpu.make_async_remote_copy(
-                results.at[name],
-                returned.at[name],
-                results_sem,
-                returned_sems.at[batch],
-                device_id=peer_at(name, -1),
-                device_id_type=MESH,
-            ).start()
+        for half in range(2):
+            results[pl.ds(batch * BATCH + half * BATCH // 2, BATCH // 2)] = packed(half)
+
+            if half == 0:
+
+                @pl.when(batch == 0)
+                def _():
+                    returned[0] = results[0]
+
+            @pl.loop(jnp.where(batch == 0, 1 - half, 0), BATCH // 2)
+            def _(step):
+                name = batch * BATCH + half * BATCH // 2 + step
+                pltpu.make_async_remote_copy(
+                    results.at[name],
+                    returned.at[name],
+                    results_sem,
+                    returned_sems.at[batch],
+                    device_id=peer_at(name, -1),
+                    device_id_type=MESH,
+                ).start()
 
     total[...] = resid_ref[...].astype(F32)
 

time: 91.4 us -> 91.3 us (level)
  no operation moved by 1% of the time
where the time goes in v5:
time: 91.3 us; the launch traced here: 91.1 us
  Pallas kernels  90.3 us (99%)
    pallas_call x1, Pallas kernels, body(): pl.pallas_call(layer_kernel, out_shape=jax.ShapeDtypeStruct((tokens, widt...  90.3 us

profile of v5, /device:TPU:1, one launch (start us, length us, event | category | flops | bytes accessed | tf_op | source)
XLA Modules:
  0.0 91.1 jit_solution(5026747697898744718)
XLA Ops:
  0.0 90.3 %layer.1 = bf16[128,2048]{1,0:T(8,128)(2,1)S(1)} custom-call(bf16[128,2048]{1,0:T(8,128)(2,1)} %stream_hbm.1, bf16[1024,256]{1,0:T(8,128)(2,1)} %projected_hbm.1, s32[8,128]{1,0:T(8,128)} %bitcast.9, bf16[4,512,512]{2,1,0:T(8,128)(2,1)} %group_hbm.1, f32[1,2048]{1,0:T(1,128)} %bitcast.7, bf16[4,512,2048]{2,1,0:T(8,128)(2,1)} %bitcast.6, f32[1,2048]{1,0:T(1,128)} %bitcast.8, ...), custom_call_target="tpu_custom_call" | custom-call | tf_op jit(solution)/shard_map/layer/pallas_call | solution.py:465
  90.3 0.8 copy.14
